TPU v7x, 32 devices: a whole 2x2x4 slice. The times are simulated.
32 devices in a mesh: sp: 4 (over z), fs: 4 (over y, x), tp: 2 (over core).
Axes of the slice: x: 2, y: 2, z: 4, core: 2. Of those that a mesh axis runs over, the one named last changes fastest.
Arguments:
- inputs: bfloat16 [4, 2048, 2048], P('fs', 'sp', 'tp'), may hold values from -6 to 6
- norm_gain: float32 [2048], replicated, may hold values from 0.1 to 1.9
- query_weight: bfloat16 [2048, 1024], P(('sp', 'fs'), 'tp'), may hold values from -0.125 to 0.125
- key_weight: bfloat16 [2048, 1024], P(('sp', 'fs'), 'tp'), may hold values from -0.125 to 0.125
- value_weight: bfloat16 [2048, 1024], P(('sp', 'fs'), 'tp'), may hold values from -0.125 to 0.125
- query_gain: float32 [64], replicated, may hold values from 0.8 to 7
- key_gain: float32 [64], replicated, may hold values from 0.8 to 7
- mix_lambda: float32 [8], replicated, may hold values from 0.3 to 0.8
- head_gain: float32 [128], replicated, may hold values from 0.1 to 1.9
- post_gate_weight: bfloat16 [2048, 2048], P(('sp', 'fs'), 'tp'), may hold values from -0.125 to 0.125
- pre_gate_weight: bfloat16 [2048, 2048], P(('sp', 'fs'), 'tp'), may hold values from -0.125 to 0.125
- inner_weight: bfloat16 [2048, 2048], P(('sp', 'fs'), 'tp'), may hold values from -0.125 to 0.125
- conv_taps: float32 [3, 2048], replicated, may hold values from -3 to 3
- attn_out_weight: bfloat16 [2048, 1024], P(('sp', 'fs'), 'tp'), may hold values from -0.109375 to 0.109375
- conv_out_weight: bfloat16 [2048, 2048], P(('sp', 'fs'), 'tp'), may hold values from -0.109375 to 0.109375
Outputs:
- mixed: bfloat16 [4, 2048, 2048], P('fs', ('sp', 'tp'))
All inputs are finite; a program needn't handle non-finite values.
Results may differ from a plain program's by a relative error of at most 0.015.
The roundings to bfloat16 on the way count: a program that leaves them out, or rounds other values in their place, can miss the bound.
Values may be sent and summed in bfloat16 or wider, within the bound.
A program may use at most 128 MiB of HBM per device.

v0:
```python
import math
import jax
import jax.numpy as jnp
from jax import lax
from jax.sharding import PartitionSpec as P

epsilon = 1e-06


def padded_2(x, sides, width):
    for axis, dim in sides:
        size, length = (lax.axis_size(axis), x.shape[dim])
        up = [(i, (i + 1) % size) for i in range(size - 1)]
        down = [(j, i) for i, j in up]
        last = lax.slice_in_dim(x, length - width, length, axis=dim)
        initial = lax.slice_in_dim(x, 0, width, axis=dim)
        before = lax.ppermute(last, axis, up)
        after = lax.ppermute(initial, axis, down)
        x = jnp.concatenate([before, x, after], axis=dim)
    return x


def scale_rows(values, gain):
    return values * lax.rsqrt(jnp.mean(values * values, axis=-1, keepdims=True) + epsilon) * gain


def project_all(normed, weights, products):
    result = []
    for member in range(len(weights)):
        if member < products:
            result.append(jnp.dot(normed, weights[member], preferred_element_type=jnp.float32))
        else:
            result.append(weights[member])
    return tuple(result)


def attention_branch(query, key, values, weight_two, query_gain, key_gain, head_gain):
    tok_rows = query.shape[0]
    vsize = head_gain.shape[0]
    half = query_gain.shape[0]
    heads = values.shape[1] // vsize
    query_normed = scale_rows(query.reshape(tok_rows, heads, 2, half), query_gain).astype(
        jnp.bfloat16
    )
    key_normed = scale_rows(key.reshape(tok_rows, heads * 2, half), key_gain).astype(jnp.bfloat16)
    key_normed = key_normed.reshape(tok_rows, heads * 2 * half)
    scale = half ** (-0.5)
    initial = (
        jnp.full((heads, 2, tok_rows), -1e30, jnp.float32),
        jnp.zeros((heads, 2, tok_rows), jnp.float32),
        jnp.zeros((heads, 2, tok_rows, vsize), jnp.float32),
    )
    carry = initial
    key_piece = lax.all_gather(key_normed, "sp", axis=0, tiled=True)
    value_piece = lax.all_gather(values, "sp", axis=0, tiled=True)
    length = key_piece.shape[0]
    block = math.gcd(length, 512)
    key_blocks = key_piece.reshape(length // block, block, heads, 2, half)
    value_blocks = value_piece.reshape(length // block, block, heads, vsize)

    def one_block(state, blocks):
        peak, total, accum = state
        key_block, value_block = blocks
        scores = (
            jnp.einsum(
                "qhjd,khjd->hjqk", query_normed, key_block, preferred_element_type=jnp.float32
            )
            * scale
        )
        new_peak = jnp.maximum(peak, jnp.max(scores, axis=-1))
        factor = jnp.exp(peak - new_peak)
        expo = jnp.exp(scores - new_peak[..., None])
        total = total * factor + jnp.sum(expo, axis=-1)
        accum = accum * factor[..., None] + jnp.einsum(
            "hjqk,khd->hjqd",
            expo.astype(jnp.bfloat16),
            value_block,
            preferred_element_type=jnp.float32,
        )
        return ((new_peak, total, accum), None)

    carry, unused = lax.scan(one_block, carry, (key_blocks, value_blocks))
    peak, total, accum = carry
    mapped = accum / total[..., None]
    head_out = mapped[:, 0] - weight_two[:, None, None] * mapped[:, 1]
    normed_out = scale_rows(head_out, head_gain).astype(jnp.bfloat16)
    return jnp.transpose(normed_out, (1, 0, 2)).reshape(tok_rows, heads * vsize)


def per_device(
    inputs,
    norm_gain,
    query_weight,
    key_weight,
    value_weight,
    query_gain,
    key_gain,
    mix_lambda,
    head_gain,
    post_gate_weight,
    pre_gate_weight,
    inner_weight,
    conv_taps,
    attn_out_weight,
    conv_out_weight,
):
    tokens = inputs[0]
    whole = lax.all_gather(tokens, "tp", axis=1, tiled=True)
    normed = scale_rows(whole.astype(jnp.float32), norm_gain).astype(jnp.bfloat16)
    heads_dev = value_weight.shape[1] // head_gain.shape[0]
    channels = post_gate_weight.shape[1]
    tp_index = lax.axis_index("tp")
    weight_two = lax.dynamic_slice_in_dim(mix_lambda, tp_index * heads_dev, heads_dev)
    taps = lax.dynamic_slice_in_dim(conv_taps, tp_index * channels, channels, 1)
    every_full = (
        lax.all_gather(query_weight, ("sp", "fs"), axis=0, tiled=True),
        lax.all_gather(key_weight, ("sp", "fs"), axis=0, tiled=True),
        lax.all_gather(value_weight, ("sp", "fs"), axis=0, tiled=True),
        lax.all_gather(post_gate_weight, ("sp", "fs"), axis=0, tiled=True),
        lax.all_gather(pre_gate_weight, ("sp", "fs"), axis=0, tiled=True),
        lax.all_gather(inner_weight, ("sp", "fs"), axis=0, tiled=True),
        lax.all_gather(attn_out_weight, ("sp", "fs"), axis=0, tiled=True),
        lax.all_gather(conv_out_weight, ("sp", "fs"), axis=0, tiled=True),
    )
    query, key, value_proj, post, pre_gate, inner, attn_out_full, conv_out_full = project_all(
        normed, every_full[0:3] + every_full[3:6] + every_full[6:8], 6
    )
    attn_hidden = attention_branch(
        query, key, value_proj.astype(jnp.bfloat16), weight_two, query_gain, key_gain, head_gain
    )
    post_mid = post.astype(jnp.bfloat16)
    post_wide = lax.optimization_barrier(post_mid).astype(jnp.float32)
    signal = (pre_gate * inner).astype(jnp.bfloat16)
    padded = padded_2(signal, (("sp", 0),), 1)
    shifted = lax.optimization_barrier(padded).astype(jnp.float32)
    filtered = taps[0] * shifted[:-2] + taps[1] * shifted[1:-1] + taps[2] * shifted[2:]
    conv_hidden = (post_wide * filtered).astype(jnp.bfloat16)
    contract = (((1,), (1,)), ((), ()))
    summed = lax.psum_scatter(
        (
            lax.dot_general(
                attn_hidden, attn_out_full, contract, preferred_element_type=jnp.float32
            )
            + lax.dot_general(
                conv_hidden, conv_out_full, contract, preferred_element_type=jnp.float32
            )
        ).astype(jnp.bfloat16),
        "tp",
        scatter_dimension=0,
        tiled=True,
    )
    return summed[None]


def solution(mesh):
    placed = (
        P("fs", "sp", "tp"),
        P(),
        P(("sp", "fs"), "tp"),
        P(("sp", "fs"), "tp"),
        P(("sp", "fs"), "tp"),
        P(),
        P(),
        P(),
        P(),
        P(("sp", "fs"), "tp"),
        P(("sp", "fs"), "tp"),
        P(("sp", "fs"), "tp"),
        P(),
        P(("sp", "fs"), "tp"),
        P(("sp", "fs"), "tp"),
    )
    return jax.shard_map(
        per_device,
        mesh=mesh,
        in_specs=placed,
        out_specs=P("fs", ("sp", "tp"), None),
        check_vma=False,
    )
```

profile of v0, /device:TPU:0, one launch (start us, length us, event | category | flops | bytes accessed | tf_op | source)
XLA Modules:
  0.0 693.1 jit_solution(11032667689516088220)
XLA Ops:
  10.1 12.1 %all-gather.33.cloned.1.call-done = bf16[1,512,2048]{2,1,0:T(8,128)(2,1)} async-done(((bf16[1,512,1024]{2,1,0:T(8,128)(2,1)}), bf16[1,512,2048]{2,1,0:T(8,128)(2,1)}) %all-gather.33.cloned.1.call-update) | async-done | bytes 2097168 | tf_op jit(solution)/shard_map/all_gather | solution.py:108
  24.4 62.1 %all-gather.13.cloned.1.call-done = bf16[2048,512]{1,0:T(8,128)(2,1)} async-done(((bf16[128,512]{1,0:T(8,128)(2,1)}), bf16[2048,512]{1,0:T(8,128)(2,1)}) %all-gather.13.cloned.1.call-update) | async-done | bytes 2097168 | tf_op jit(solution)/shard_map/all_gather | solution.py:117
  90.6 57.9 %all-gather.19.cloned.1.call-done = bf16[2048,512]{1,0:T(8,128)(2,1)} async-done(((bf16[128,512]{1,0:T(8,128)(2,1)}), bf16[2048,512]{1,0:T(8,128)(2,1)}) %all-gather.19.cloned.1.call-update) | async-done | bytes 2097168 | tf_op jit(solution)/shard_map/all_gather | solution.py:118
  157.1 53.3 %all-gather.17.cloned.1.call-done = bf16[2048,512]{1,0:T(8,128)(2,1)} async-done(((bf16[128,512]{1,0:T(8,128)(2,1)}), bf16[2048,512]{1,0:T(8,128)(2,1)}) %all-gather.17.cloned.1.call-update) | async-done | bytes 2097168 | tf_op jit(solution)/shard_map/all_gather | solution.py:116
  214.3 42.0 %all-gather.15.cloned.1.call-done = bf16[2048,512]{0,1:T(8,128)(2,1)} async-done(((bf16[512,512]{0,1:T(8,128)(2,1)}), bf16[2048,512]{0,1:T(8,128)(2,1)}) %all-gather.15.cloned.1.call-update) | async-done | bytes 2097168 | tf_op jit(solution)/shard_map/all_gather | solution.py:54
  264.2 38.0 %all-gather.21.cloned.1.call-done = bf16[2048,512]{1,0:T(8,128)(2,1)} async-done(((bf16[512,512]{1,0:T(8,128)(2,1)}), bf16[2048,512]{1,0:T(8,128)(2,1)}) %all-gather.21.cloned.1.call-update) | async-done | bytes 2097168 | tf_op jit(solution)/shard_map/all_gather | solution.py:55
  306.2 59.2 %while.15 = (s32[]{:T(128)}, f32[4,2,512]{2,1,0:T(2,128)S(1)}, f32[4,2,512]{2,1,0:T(2,128)S(1)}, f32[4,2,512,128]{3,2,1,0:T(8,128)S(1)}, bf16[4,512,4,2,64]{1,4,...) while((s32[]{:T(128)}, f32[4,2,512]{2,1,0:T(2,128)S(1)}, ...), condition=%wide.region_6.7_spmd.clone, body=%wide.region_3.6_spmd.clone.sunk | while | flops 823676928 | bytes 65798792 | solution.py:82
  306.2 5.6 bitcast_reduce_fusion.3
  311.9 5.1 fusion.62
  321.0 5.6 bitcast_reduce_fusion.3
  335.8 5.6 bitcast_reduce_fusion.3
  350.5 5.8 bitcast_reduce_fusion.3
  356.3 5.0 fusion.62
  370.1 9.3 %all-gather.27.cloned.1.call-done = bf16[2048,1024]{1,0:T(8,128)(2,1)} async-done(((bf16[128,1024]{1,0:T(8,128)(2,1)}), bf16[2048,1024]{1,0:T(8,128)(2,1)}) %all-gather.27.cloned.1.call-update) | async-done | bytes 4194320 | tf_op jit(solution)/shard_map/all_gather | solution.py:120
  379.4 5.9 fusion.34
  385.3 71.1 %all-gather.29.cloned.1.call-done = bf16[2048,1024]{1,0:T(8,128)(2,1)} async-done(((bf16[128,1024]{1,0:T(8,128)(2,1)}), bf16[2048,1024]{1,0:T(8,128)(2,1)}) %all-gather.29.cloned.1.call-update) | async-done | bytes 4194320 | tf_op jit(solution)/shard_map/all_gather | solution.py:121
  456.4 5.2 multiply_convert_fusion
  467.5 65.9 %all-gather.25.cloned.1.call-done = bf16[2048,1024]{1,0:T(8,128)(2,1)} async-done(((bf16[128,1024]{1,0:T(8,128)(2,1)}), bf16[2048,1024]{1,0:T(8,128)(2,1)}) %all-gather.25.cloned.1.call-update) | async-done | bytes 4194320 | tf_op jit(solution)/shard_map/all_gather | solution.py:119
  533.4 5.7 convolution_convert_fusion
  539.6 70.6 %all-gather.31.cloned.1.call-done = bf16[2048,1024]{1,0:T(8,128)(2,1)} async-done(((bf16[128,1024]{1,0:T(8,128)(2,1)}), bf16[2048,1024]{1,0:T(8,128)(2,1)}) %all-gather.31.cloned.1.call-update) | async-done | bytes 4194320 | tf_op jit(solution)/shard_map/all_gather | solution.py:123
  610.2 7.1 %fusion.24 = f32[512,2048]{1,0:T(8,128)} fusion(bf16[2048,1024]{1,0:T(8,128)(2,1)} %all-gather.31.cloned.1.call-done, f32[514,1024]{1,0:T(8,128)S(1)} %convert_element_type.49, bf16[512,1024]{1,0:T(8,128)(2,1)} %convolution_convert_fusion, f32[1024]{0:T(1024)S(1)} %bitcast.100, f32[1024]{0:T(1024)S(1)} %bitcast.99, f32[1024]{0:T(1024)S(1)} %bitcast.98), kind=kOutput, calls=%fused_computation.39 | convolution fusion | flops 2151677952 | bytes 15740928 | tf_op jit(solution)/shard_map/dot_general | solution.py:144
  617.4 54.7 %all-gather.23.cloned.1.call-done = bf16[2048,512]{1,0:T(8,128)(2,1)} async-done(((bf16[128,512]{1,0:T(8,128)(2,1)}), bf16[2048,512]{1,0:T(8,128)(2,1)}) %all-gather.23.cloned.1.call-update) | async-done | bytes 2097168 | tf_op jit(solution)/shard_map/all_gather | solution.py:122
  672.0 5.5 add_convert_fusion
  677.6 8.7 %reduce-scatter.2.cloned.1.call-done = bf16[256,2048]{1,0:T(8,128)(2,1)} async-done(((bf16[512,2048]{1,0:T(8,128)(2,1)}), bf16[256,2048]{1,0:T(8,128)(2,1)}) %reduce-scatter.2.cloned.1.call-update) | async-done | bytes 1048592 | tf_op jit(solution)/shard_map/reduce_scatter | solution.py:139
  (102 shorter events, 71.2 us)
Async XLA Ops:
  6.5 80.0 %copy-start.7 = (f32[2048]{0:T(1024)S(1)}, f32[2048]{0:T(1024)}, u32[]{:S(2)}) copy-start(f32[2048]{0:T(1024)} %param.18) | copy-start | bytes 24580
  6.5 15.7 %all-gather.33.cloned.1.call-start = ((), (), s32[]{:S(2)}) async-start(), calls=%async_computation.12 | async-start | bytes 3145728 | tf_op jit(solution)/shard_map/all_gather | solution.py:108
  7.3 79.3 %all-gather.13.cloned.1.call-start = ((), (), s32[]{:S(2)}) async-start(), calls=%async_computation.1 | async-start | bytes 2228224 | tf_op jit(solution)/shard_map/all_gather | solution.py:117
  8.0 140.5 %all-gather.19.cloned.1.call-start = ((), (), s32[]{:S(2)}) async-start(), calls=%async_computation.4 | async-start | bytes 2228224 | tf_op jit(solution)/shard_map/all_gather | solution.py:118
  8.7 201.6 %all-gather.17.cloned.1.call-start = ((), (), s32[]{:S(2)}) async-start(), calls=%async_computation.3 | async-start | bytes 2228224 | tf_op jit(solution)/shard_map/all_gather | solution.py:116
  9.3 247.0 %all-gather.15.cloned.1.call-start = ((), (), s32[]{:S(2)}) async-start(), calls=%async_computation.2 | async-start | bytes 2621440 | tf_op jit(solution)/shard_map/all_gather | solution.py:54
  22.2 64.4 %copy-start.1 = (bf16[1,512,2048]{2,1,0:T(8,128)(2,1)S(1)}, bf16[1,512,2048]{2,1,0:T(8,128)(2,1)}, u32[]{:S(2)}) copy-start(bf16[1,512,2048]{2,1,0:T(8,128)(2,1)} %all-gather.33.cloned.1.call-done) | copy-start | bytes 6291460
  90.6 65.5 %copy-start.8 = (f32[8]{0:T(128)S(1)}, f32[8]{0:T(128)}, u32[]{:S(2)}) copy-start(f32[8]{0:T(128)} %param.24) | copy-start | bytes 100
  90.6 211.6 %all-gather.21.cloned.1.call-start = ((), (), s32[]{:S(2)}) async-start(), calls=%async_computation.5 | async-start | bytes 2621440 | tf_op jit(solution)/shard_map/all_gather | solution.py:55
  152.3 227.1 %all-gather.27.cloned.1.call-start = ((), (), s32[]{:S(2)}) async-start(), calls=%async_computation.8 | async-start | bytes 4456448 | tf_op jit(solution)/shard_map/all_gather | solution.py:120
  153.0 303.4 %all-gather.29.cloned.1.call-start = ((), (), s32[]{:S(2)}) async-start(), calls=%async_computation.9 | async-start | bytes 4456448 | tf_op jit(solution)/shard_map/all_gather | solution.py:121
  153.8 379.6 %all-gather.25.cloned.1.call-start = ((), (), s32[]{:S(2)}) async-start(), calls=%async_computation.7 | async-start | bytes 4456448 | tf_op jit(solution)/shard_map/all_gather | solution.py:119
  154.5 455.7 %all-gather.31.cloned.1.call-start = ((), (), s32[]{:S(2)}) async-start(), calls=%async_computation.10 | async-start | bytes 4456448 | tf_op jit(solution)/shard_map/all_gather | solution.py:123
  155.1 516.9 %all-gather.23.cloned.1.call-start = ((), (), s32[]{:S(2)}) async-start(), calls=%async_computation.6 | async-start | bytes 2228224 | tf_op jit(solution)/shard_map/all_gather | solution.py:122
  155.8 530.4 %reduce-scatter.2.cloned.1.call-start = ((), (), s32[]{:S(2)}) async-start(), calls=%async_computation.11 | async-start | bytes 3145728 | tf_op jit(solution)/shard_map/reduce_scatter | solution.py:139
  157.1 57.0 %copy-start.5 = (f32[64]{0:T(128)S(1)}, f32[64]{0:T(128)}, u32[]{:S(2)}) copy-start(f32[64]{0:T(128)} %param.22) | copy-start | bytes 772
  311.8 6.4 copy-start
  326.7 6.3 copy-start
  341.4 6.3 copy-start
  356.3 6.3 copy-start
  369.2 10.2 %copy-start.2 = (bf16[1,512,2048]{2,1,0:T(8,128)(2,1)S(1)}, bf16[1,512,2048]{2,1,0:T(8,128)(2,1)}, u32[]{:S(2)}) copy-start(bf16[1,512,2048]{2,1,0:T(8,128)(2,1)} %all-gather.33.cloned.1.call-done) | copy-start | bytes 6291460
  462.6 76.5 %collective-permute-start = (bf16[1,1024]{1,0:T(2,128)(2,1)S(1)}, bf16[1,1024]{1,0:T(2,128)(2,1)S(1)}, u32[]{:S(2)}, u32[]{:S(2)}) collective-permute-start(bf16[1,1024]{1,0:T(2,128)(2,1)S(1)} %get-tuple-element.101), channel_id=1, source_target_pairs={{0,8},{8,16},{16,24},{1,9},{9,17},{17,25},{2,10},{10,18},{18,26},{... | collective-permute-start | bytes 6152 | tf_op jit(solution)/shard_map/ppermute | solution.py:17
  466.0 73.1 %collective-permute-start.1 = (bf16[1,1024]{1,0:T(2,128)(2,1)S(1)}, bf16[1,1024]{1,0:T(2,128)(2,1)S(1)}, u32[]{:S(2)}, u32[]{:S(2)}) collective-permute-start(bf16[1,1024]{1,0:T(2,128)(2,1)S(1)} %get-tuple-element.102), channel_id=1, source_target_pairs={{8,0},{16,8},{24,16},{9,1},{17,9},{25,17},{10,2},{18,10},{26,18},{... | collective-permute-start | bytes 6152 | tf_op jit(solution)/shard_map/ppermute | solution.py:18
  533.4 5.7 copy-start.4
  (2 other events, 1.6 us)
Sparse Core Ops, SparseCore 0:
  8.9 13.2 all-gather.32
  25.0 61.5 all-gather.12
  89.3 59.1 all-gather.18
  151.2 59.1 all-gather.16
  211.8 44.4 all-gather.14
  257.7 44.4 all-gather.20
  305.0 74.3 all-gather.26
  382.2 74.1 all-gather.28
  459.2 74.1 all-gather.24
  536.0 74.1 all-gather.30
  613.0 58.9 all-gather.22
  677.7 8.5 reduce-scatter.1
where the time goes:
time: 694 us; the launch traced here: 693 us
  waiting for transfers between devices  552 us (80%)
  matrix products  73.6 us (11%)
  other arithmetic  26.6 us (4%)
  local copies, waits for them, and re-layouts  21.7 us (3%)
  between operations  13.8 us (2%)
    all_gather x1, waiting for transfers between devices, per_device(): lax.all_gather(inner_weight, ('sp', 'fs'), axis=0, tiled=True)  71.1 us
    all_gather x1, waiting for transfers between devices, per_device(): lax.all_gather(conv_out_weight, ('sp', 'fs'), axis=0, tiled=True)  70.6 us
    all_gather x1, waiting for transfers between devices, per_device(): lax.all_gather(post_gate_weight, ('sp', 'fs'), axis=0, tiled=True)  65.9 us
    all_gather x1, waiting for transfers between devices, per_device(): lax.all_gather(key_weight, ('sp', 'fs'), axis=0, tiled=True)  62.1 us
    all_gather x1, waiting for transfers between devices, per_device(): lax.all_gather(value_weight, ('sp', 'fs'), axis=0, tiled=True)  57.9 us
    all_gather x1, waiting for transfers between devices, per_device(): lax.all_gather(attn_out_weight, ('sp', 'fs'), axis=0, tiled=True)  54.7 us
    all_gather x1, waiting for transfers between devices, per_device(): lax.all_gather(query_weight, ('sp', 'fs'), axis=0, tiled=True)  53.3 us
    all_gather x1, waiting for transfers between devices, attention_branch(): key_piece = lax.all_gather(key_normed, 'sp', axis=0, tiled=True)  42 us
  transfers between devices with their start and end apart: 14, of which 12 were waited for; matrix products, arithmetic and copies ran while one was open for 17% of the time, Pallas kernels for 0%

commit v1 on v0

--- a/solution.py
+++ b/solution.py
@@ -51,7 +51,15 @@
         jnp.zeros((heads, 2, tok_rows, vsize), jnp.float32),
     )
     carry = initial
-    key_piece = lax.all_gather(key_normed, "sp", axis=0, tiled=True)
+    degree = lax.axis_size("sp")
+    mixed_arr = sorted(((tick, (tick + 1) % degree) for tick in range(degree)))
+    response = key_normed
+    entries = [response]
+    for q in tuple(range(1, degree)):
+        response = lax.ppermute(response, axis_name="sp", perm=mixed_arr)
+        entries.insert(0, response)
+    built = jnp.concatenate(entries, axis=0)
+    key_piece = jnp.roll(built, (lax.axis_index("sp") + 1) * key_normed.shape[0], axis=0)
     value_piece = lax.all_gather(values, "sp", axis=0, tiled=True)
     length = key_piece.shape[0]
     block = math.gcd(length, 512)

time: 694 us -> 658 us (0.948)
  waiting for transfers between devices: 552 us -> 509 us
    all_gather x1 -> x0, waiting for transfers between devices: 42 us -> none  [attention_branch(): key_piece = lax.all_gather(key_normed, 'sp', axis=0, tiled=True)]
    ppermute x0 -> x3, waiting for transfers between devices: none -> 27.2 us  [attention_branch(): response = lax.ppermute(response, axis_name='sp', perm=mixed_arr)]
    all_gather x1, waiting for transfers between devices: 53.3 us -> 39 us  [per_device(): lax.all_gather(query_weight, ('sp', 'fs'), axis=0, tiled=True)]
    all_gather x1, waiting for transfers between devices: 38 us -> 27.6 us  [attention_branch(): value_piece = lax.all_gather(values, 'sp', axis=0, tiled=True)]
    all_gather x1, waiting for transfers between devices: 62.1 us -> 54.7 us  [per_device(): lax.all_gather(key_weight, ('sp', 'fs'), axis=0, tiled=True)]
  transfers between devices with their start and end apart: 14 -> 16, of which waited for: 12 -> 13; matrix products, arithmetic and copies ran while one was open for 17% -> 18% of each run, Pallas kernels for 0% -> 0%
where the time goes in v1:
time: 658 us; the launch traced here: 657 us
  waiting for transfers between devices  509 us (77%)
  matrix products  74.3 us (11%)
  local copies, waits for them, and re-layouts  27.2 us (4%)
  other arithmetic  25.7 us (4%)
  between operations  13.6 us (2%)
  starting transfers between devices  6.8 us (1%)
    all_gather x1, waiting for transfers between devices, per_device(): lax.all_gather(inner_weight, ('sp', 'fs'), axis=0, tiled=True)  71.1 us
    all_gather x1, waiting for transfers between devices, per_device(): lax.all_gather(conv_out_weight, ('sp', 'fs'), axis=0, tiled=True)  70.7 us
    all_gather x1, waiting for transfers between devices, per_device(): lax.all_gather(post_gate_weight, ('sp', 'fs'), axis=0, tiled=True)  65.8 us
    all_gather x1, waiting for transfers between devices, per_device(): lax.all_gather(value_weight, ('sp', 'fs'), axis=0, tiled=True)  62.2 us
    all_gather x1, waiting for transfers between devices, per_device(): lax.all_gather(key_weight, ('sp', 'fs'), axis=0, tiled=True)  54.7 us
    all_gather x1, waiting for transfers between devices, per_device(): lax.all_gather(attn_out_weight, ('sp', 'fs'), axis=0, tiled=True)  54.5 us
    all_gather x1, waiting for transfers between devices, per_device(): lax.all_gather(query_weight, ('sp', 'fs'), axis=0, tiled=True)  39 us
    dot_general x6, matrix products, project_all(): jnp.dot(normed, weights[member], preferred_element_type=jnp.float32)  27.8 us
  transfers between devices with their start and end apart: 16, of which 13 were waited for; matrix products, arithmetic and copies ran while one was open for 18% of the time, Pallas kernels for 0%

profile of v1, /device:TPU:0, one launch (start us, length us, event | category | flops | bytes accessed | tf_op | source)
XLA Modules:
  0.0 656.9 jit_solution(4951756206929355065)
XLA Ops:
  9.4 12.8 %all-gather.30.cloned.1.call-done = bf16[1,512,2048]{2,1,0:T(8,128)(2,1)} async-done(((bf16[1,512,1024]{2,1,0:T(8,128)(2,1)}), bf16[1,512,2048]{2,1,0:T(8,128)(2,1)}) %all-gather.30.cloned.1.call-update) | async-done | bytes 2097168 | tf_op jit(solution)/shard_map/all_gather | solution.py:116
  24.3 62.2 %all-gather.16.cloned.1.call-done = bf16[2048,512]{1,0:T(8,128)(2,1)} async-done(((bf16[128,512]{1,0:T(8,128)(2,1)}), bf16[2048,512]{1,0:T(8,128)(2,1)}) %all-gather.16.cloned.1.call-update) | async-done | bytes 2097168 | tf_op jit(solution)/shard_map/all_gather | solution.py:126
  93.9 54.7 %all-gather.12.cloned.1.call-done = bf16[2048,512]{1,0:T(8,128)(2,1)} async-done(((bf16[128,512]{1,0:T(8,128)(2,1)}), bf16[2048,512]{1,0:T(8,128)(2,1)}) %all-gather.12.cloned.1.call-update) | async-done | bytes 2097168 | tf_op jit(solution)/shard_map/all_gather | solution.py:125
  153.3 15.0 %collective-permute-done = bf16[512,512]{0,1:T(8,128)(2,1)S(1)} collective-permute-done((bf16[512,512]{0,1:T(8,128)(2,1)S(1)}, bf16[512,512]{0,1:T(8,128)(2,1)S(1)}, u32[]{:S(2)}, u32[]{:S(2)}) %collective-permute-start) | collective-permute-done | bytes 524320 | tf_op jit(solution)/shard_map/ppermute | solution.py:59
  169.4 12.2 %collective-permute-done.1 = bf16[512,512]{0,1:T(8,128)(2,1)} collective-permute-done((bf16[512,512]{0,1:T(8,128)(2,1)S(1)}, bf16[512,512]{0,1:T(8,128)(2,1)}, u32[]{:S(2)}, u32[]{:S(2)}) %collective-permute-start.1) | collective-permute-done | bytes 524320 | tf_op jit(solution)/shard_map/ppermute | solution.py:59
  181.6 39.0 %all-gather.14.cloned.1.call-done = bf16[2048,512]{1,0:T(8,128)(2,1)} async-done(((bf16[128,512]{1,0:T(8,128)(2,1)}), bf16[2048,512]{1,0:T(8,128)(2,1)}) %all-gather.14.cloned.1.call-update) | async-done | bytes 2097168 | tf_op jit(solution)/shard_map/all_gather | solution.py:124
  238.9 27.6 %all-gather.18.cloned.1.call-done = bf16[2048,512]{1,0:T(8,128)(2,1)} async-done(((bf16[512,512]{1,0:T(8,128)(2,1)}), bf16[2048,512]{1,0:T(8,128)(2,1)}) %all-gather.18.cloned.1.call-update) | async-done | bytes 2097168 | tf_op jit(solution)/shard_map/all_gather | solution.py:63
  270.5 59.3 %while.15 = (s32[]{:T(128)}, f32[4,2,512]{2,1,0:T(2,128)S(1)}, f32[4,2,512]{2,1,0:T(2,128)S(1)}, f32[4,2,512,128]{3,2,1,0:T(8,128)S(1)}, bf16[4,512,4,2,64]{1,4,...) while((s32[]{:T(128)}, f32[4,2,512]{2,1,0:T(2,128)S(1)}, ...), condition=%wide.region_6.7_spmd.clone, body=%wide.region_3.6_spmd.clone.sunk | while | flops 823676928 | bytes 65798792 | solution.py:90
  270.5 5.6 bitcast_reduce_fusion.3
  276.2 5.1 fusion.62
  285.3 5.6 bitcast_reduce_fusion.3
  300.1 5.6 bitcast_reduce_fusion.3
  314.8 5.8 bitcast_reduce_fusion.3
  334.1 9.4 %all-gather.24.cloned.1.call-done = bf16[2048,1024]{1,0:T(8,128)(2,1)} async-done(((bf16[128,1024]{1,0:T(8,128)(2,1)}), bf16[2048,1024]{1,0:T(8,128)(2,1)}) %all-gather.24.cloned.1.call-update) | async-done | bytes 4194320 | tf_op jit(solution)/shard_map/all_gather | solution.py:128
  343.5 5.9 fusion.34
  349.5 71.1 %all-gather.26.cloned.1.call-done = bf16[2048,1024]{1,0:T(8,128)(2,1)} async-done(((bf16[128,1024]{1,0:T(8,128)(2,1)}), bf16[2048,1024]{1,0:T(8,128)(2,1)}) %all-gather.26.cloned.1.call-update) | async-done | bytes 4194320 | tf_op jit(solution)/shard_map/all_gather | solution.py:129
  420.5 5.2 multiply_convert_fusion
  431.7 65.8 %all-gather.22.cloned.1.call-done = bf16[2048,1024]{1,0:T(8,128)(2,1)} async-done(((bf16[128,1024]{1,0:T(8,128)(2,1)}), bf16[2048,1024]{1,0:T(8,128)(2,1)}) %all-gather.22.cloned.1.call-update) | async-done | bytes 4194320 | tf_op jit(solution)/shard_map/all_gather | solution.py:127
  497.5 5.7 convolution_convert_fusion
  503.8 70.7 %all-gather.28.cloned.1.call-done = bf16[2048,1024]{1,0:T(8,128)(2,1)} async-done(((bf16[128,1024]{1,0:T(8,128)(2,1)}), bf16[2048,1024]{1,0:T(8,128)(2,1)}) %all-gather.28.cloned.1.call-update) | async-done | bytes 4194320 | tf_op jit(solution)/shard_map/all_gather | solution.py:131
  574.5 7.1 %fusion.24 = f32[512,2048]{1,0:T(8,128)} fusion(bf16[2048,1024]{1,0:T(8,128)(2,1)} %all-gather.28.cloned.1.call-done, f32[514,1024]{1,0:T(8,128)S(1)} %convert_element_type.49, bf16[512,1024]{1,0:T(8,128)(2,1)} %convolution_convert_fusion, f32[1024]{0:T(1024)S(1)} %bitcast.100, f32[1024]{0:T(1024)S(1)} %bitcast.99, f32[1024]{0:T(1024)S(1)} %bitcast.98), kind=kOutput, calls=%fused_computation.39 | convolution fusion | flops 2151677952 | bytes 15740928 | tf_op jit(solution)/shard_map/dot_general | solution.py:152
  581.6 54.5 %all-gather.20.cloned.1.call-done = bf16[2048,512]{1,0:T(8,128)(2,1)} async-done(((bf16[128,512]{1,0:T(8,128)(2,1)}), bf16[2048,512]{1,0:T(8,128)(2,1)}) %all-gather.20.cloned.1.call-update) | async-done | bytes 2097168 | tf_op jit(solution)/shard_map/all_gather | solution.py:130
  636.2 5.5 add_convert_fusion
  641.7 8.7 %reduce-scatter.2.cloned.1.call-done = bf16[256,2048]{1,0:T(8,128)(2,1)} async-done(((bf16[512,2048]{1,0:T(8,128)(2,1)}), bf16[256,2048]{1,0:T(8,128)(2,1)}) %reduce-scatter.2.cloned.1.call-update) | async-done | bytes 1048592 | tf_op jit(solution)/shard_map/reduce_scatter | solution.py:147
  (120 shorter events, 82.1 us)
Async XLA Ops:
  6.5 80.0 %copy-start.10 = (f32[2048]{0:T(1024)S(1)}, f32[2048]{0:T(1024)}, u32[]{:S(2)}) copy-start(f32[2048]{0:T(1024)} %param.18) | copy-start | bytes 24580
  6.5 15.7 %all-gather.30.cloned.1.call-start = ((), (), s32[]{:S(2)}) async-start(), calls=%async_computation.11 | async-start | bytes 3145728 | tf_op jit(solution)/shard_map/all_gather | solution.py:116
  7.3 79.3 %all-gather.16.cloned.1.call-start = ((), (), s32[]{:S(2)}) async-start(), calls=%async_computation.3 | async-start | bytes 2228224 | tf_op jit(solution)/shard_map/all_gather | solution.py:126
  8.0 140.5 %all-gather.12.cloned.1.call-start = ((), (), s32[]{:S(2)}) async-start(), calls=%async_computation.1 | async-start | bytes 2228224 | tf_op jit(solution)/shard_map/all_gather | solution.py:125
  8.7 211.8 %all-gather.14.cloned.1.call-start = ((), (), s32[]{:S(2)}) async-start(), calls=%async_computation.2 | async-start | bytes 2228224 | tf_op jit(solution)/shard_map/all_gather | solution.py:124
  9.3 257.2 %all-gather.18.cloned.1.call-start = ((), (), s32[]{:S(2)}) async-start(), calls=%async_computation.4 | async-start | bytes 2621440 | tf_op jit(solution)/shard_map/all_gather | solution.py:63
  24.3 69.5 %copy-start.9 = (f32[64]{0:T(128)S(1)}, f32[64]{0:T(128)}, u32[]{:S(2)}) copy-start(f32[64]{0:T(128)} %param.23) | copy-start | bytes 772
  24.3 124.3 %copy-start.1 = (bf16[1,512,2048]{2,1,0:T(8,128)(2,1)S(1)}, bf16[1,512,2048]{2,1,0:T(8,128)(2,1)}, u32[]{:S(2)}) copy-start(bf16[1,512,2048]{2,1,0:T(8,128)(2,1)} %all-gather.30.cloned.1.call-done) | copy-start | bytes 6291460
  90.9 252.6 %all-gather.24.cloned.1.call-start = ((), (), s32[]{:S(2)}) async-start(), calls=%async_computation.7 | async-start | bytes 4456448 | tf_op jit(solution)/shard_map/all_gather | solution.py:128
  91.5 329.0 %all-gather.26.cloned.1.call-start = ((), (), s32[]{:S(2)}) async-start(), calls=%async_computation.8 | async-start | bytes 4456448 | tf_op jit(solution)/shard_map/all_gather | solution.py:129
  92.2 405.3 %all-gather.22.cloned.1.call-start = ((), (), s32[]{:S(2)}) async-start(), calls=%async_computation.6 | async-start | bytes 4456448 | tf_op jit(solution)/shard_map/all_gather | solution.py:127
  93.0 481.5 %all-gather.28.cloned.1.call-start = ((), (), s32[]{:S(2)}) async-start(), calls=%async_computation.9 | async-start | bytes 4456448 | tf_op jit(solution)/shard_map/all_gather | solution.py:131
  93.7 542.4 %all-gather.20.cloned.1.call-start = ((), (), s32[]{:S(2)}) async-start(), calls=%async_computation.5 | async-start | bytes 2228224 | tf_op jit(solution)/shard_map/all_gather | solution.py:130
  93.9 74.5 %copy-start.11 = (f32[8]{0:T(128)S(1)}, f32[8]{0:T(128)}, u32[]{:S(2)}) copy-start(f32[8]{0:T(128)} %param.24) | copy-start | bytes 100
  151.8 16.5 %collective-permute-start = (bf16[512,512]{0,1:T(8,128)(2,1)S(1)}, bf16[512,512]{0,1:T(8,128)(2,1)S(1)}, u32[]{:S(2)}, u32[]{:S(2)}) collective-permute-start(bf16[512,512]{0,1:T(8,128)(2,1)S(1)} %fusion.29), channel_id=1, source_target_pairs={{0,8},{8,16},{16,24},{24,0},{1,9},{9,17},{17,25},{25,1},{2,10},{10... | collective-permute-start | bytes 1572872 | tf_op jit(solution)/shard_map/ppermute | solution.py:59
  168.2 56.0 %copy-start.3 = (bf16[512,512]{0,1:T(8,128)(2,1)}, bf16[512,512]{0,1:T(8,128)(2,1)S(1)}, u32[]{:S(2)}) copy-start(bf16[512,512]{0,1:T(8,128)(2,1)S(1)} %collective-permute-done) | copy-start | bytes 1572868
  168.3 13.4 %collective-permute-start.1 = (bf16[512,512]{0,1:T(8,128)(2,1)S(1)}, bf16[512,512]{0,1:T(8,128)(2,1)}, u32[]{:S(2)}, u32[]{:S(2)}) collective-permute-start(bf16[512,512]{0,1:T(8,128)(2,1)S(1)} %collective-permute-done), channel_id=1, source_target_pairs={{0,8},{8,16},{16,24},{24,0},{1,9},{9,17},{17,25},{25,1},{2,10},{10... | collective-permute-start | bytes 1572872 | tf_op jit(solution)/shard_map/ppermute | solution.py:59
  168.3 482.1 %reduce-scatter.2.cloned.1.call-start = ((), (), s32[]{:S(2)}) async-start(), calls=%async_computation.10 | async-start | bytes 3145728 | tf_op jit(solution)/shard_map/reduce_scatter | solution.py:147
  169.4 54.9 %copy-start.7 = (f32[64]{0:T(128)S(1)}, f32[64]{0:T(128)}, u32[]{:S(2)}) copy-start(f32[64]{0:T(128)} %param.22) | copy-start | bytes 772
  181.6 42.9 %collective-permute-start.2 = (bf16[512,512]{0,1:T(8,128)(2,1)}, bf16[512,512]{0,1:T(8,128)(2,1)}, u32[]{:S(2)}, u32[]{:S(2)}) collective-permute-start(bf16[512,512]{0,1:T(8,128)(2,1)} %collective-permute-done.1), channel_id=1, source_target_pairs={{0,8},{8,16},{16,24},{24,0},{1,9},{9,17},{17,25},{25,1},{2,10},{10... | collective-permute-start | bytes 1572872 | tf_op jit(solution)/shard_map/ppermute | solution.py:59
  276.1 6.3 copy-start
  333.5 10.0 %copy-start.2 = (bf16[1,512,2048]{2,1,0:T(8,128)(2,1)S(1)}, bf16[1,512,2048]{2,1,0:T(8,128)(2,1)}, u32[]{:S(2)}) copy-start(bf16[1,512,2048]{2,1,0:T(8,128)(2,1)} %all-gather.30.cloned.1.call-done) | copy-start | bytes 6291460
  426.8 76.5 %collective-permute-start.3 = (bf16[1,1024]{1,0:T(2,128)(2,1)S(1)}, bf16[1,1024]{1,0:T(2,128)(2,1)S(1)}, u32[]{:S(2)}, u32[]{:S(2)}) collective-permute-start(bf16[1,1024]{1,0:T(2,128)(2,1)S(1)} %get-tuple-element.101), channel_id=1, source_target_pairs={{0,8},{8,16},{16,24},{1,9},{9,17},{17,25},{2,10},{10,18},{18,26},{... | collective-permute-start | bytes 6152 | tf_op jit(solution)/shard_map/ppermute | solution.py:17
  430.2 73.1 %collective-permute-start.4 = (bf16[1,1024]{1,0:T(2,128)(2,1)S(1)}, bf16[1,1024]{1,0:T(2,128)(2,1)S(1)}, u32[]{:S(2)}, u32[]{:S(2)}) collective-permute-start(bf16[1,1024]{1,0:T(2,128)(2,1)S(1)} %get-tuple-element.102), channel_id=1, source_target_pairs={{8,0},{16,8},{24,16},{9,1},{17,9},{25,17},{10,2},{18,10},{26,18},{... | collective-permute-start | bytes 6152 | tf_op jit(solution)/shard_map/ppermute | solution.py:18
  (7 other events, 30.3 us)
Sparse Core Ops, SparseCore 0:
  8.9 13.2 all-gather.29
  25.0 61.5 all-gather.15
  89.3 59.1 all-gather.11
  151.2 69.3 all-gather.13
  222.0 44.4 all-gather.17
  269.1 74.3 all-gather.23
  346.3 74.1 all-gather.25
  423.3 74.1 all-gather.21
  500.3 74.1 all-gather.27
  577.1 58.9 all-gather.19
  641.8 8.5 reduce-scatter.1
